TPU v7x, 32 devices: a whole 2x2x4 slice. The times are simulated.
32 devices in a mesh: ep: 16 (over z, y, x), tp: 2 (over core).
Axes of the slice: x: 2, y: 2, z: 4, core: 2. Of those that a mesh axis runs over, the one named last changes fastest.
Arguments:
- tokens: bfloat16 [2048, 2048], P('ep'), may hold values from -6 to 6
- cotangent: bfloat16 [2048, 2048], P('ep'), may hold values from -0.625 to 0.625
- routes: int32 [2048, 2], P('ep'), may hold values from 0 to 15, as said below
- router_group: bfloat16 [2048, 4], replicated, may hold values from -0.125 to 0.125
- router_expert: bfloat16 [2048, 16], replicated, may hold values from -0.125 to 0.125
- gate_proj: bfloat16 [16, 2048, 512], P('ep', None, 'tp'), may hold values from -0.125 to 0.125
- up_proj: bfloat16 [16, 2048, 512], P('ep', None, 'tp'), may hold values from -0.125 to 0.125
- down_proj: bfloat16 [16, 512, 2048], P('ep', 'tp'), may hold values from -0.25 to 0.25
Outputs:
- token_grad: bfloat16 [2048, 2048], P('ep', 'tp')
- gate_grad: bfloat16 [16, 2048, 512], P('ep', None, 'tp')
- up_grad: bfloat16 [16, 2048, 512], P('ep', None, 'tp')
- down_grad: bfloat16 [16, 512, 2048], P('ep', 'tp')
- gate_rows: float32 [16, 2048], P('ep')
- up_rows: float32 [16, 2048], P('ep')
- down_rows: float32 [16, 512], P('ep', 'tp')
- router_expert_grad: float32 [2048, 16], P(('ep', 'tp'))
- router_group_grad: float32 [2048, 4], P(('ep', 'tp'))
- router_rows: float32 [2048], P(('ep', 'tp'))
Inputs may be any that keep to these rules, and one draw needn't show every extreme that they name: `routes`: the 2 entries of a row are different experts of one group: their quotients by 4 are equal. Among the rows of one device no expert is named more than 32 times, and the experts of one group, the same for all devices, are each named exactly 32 times by the rows of every device.
All inputs are finite; a program needn't handle non-finite values.
Results may differ from a plain program's by a relative error of at most 0.014.
Values may be sent and summed in bfloat16 or wider, within the bound.
A program may use at most 64 MiB of HBM per device.

v0:
```python
import jax
import jax.numpy as jnp
from jax import lax
from jax.sharding import PartitionSpec as P


def contract_rows(left_side, right_side):
    return lax.dot_general(
        left_side, right_side, (((0,), (0,)), ((), ())), preferred_element_type=jnp.float32
    )


def contract_cols(left_side, right_side):
    return lax.dot_general(
        left_side, right_side, (((1,), (1,)), ((), ())), preferred_element_type=jnp.float32
    )


def router_forward(tokens, routes, router_group, router_expert):
    groups = router_group.shape[1]
    experts = router_expert.shape[1]
    group_logits = jnp.dot(tokens, router_group, preferred_element_type=jnp.float32)
    expert_logits = jnp.dot(tokens, router_expert, preferred_element_type=jnp.float32)
    group_exp = jnp.exp(group_logits)
    group_prob = group_exp / jnp.sum(group_exp, axis=1, keepdims=True)
    chosen_group = routes[:, 0] // (experts // groups)
    group_onehot = (chosen_group[:, None] == jnp.arange(groups, dtype=jnp.int32)[None, :]).astype(
        jnp.float32
    )
    picked = jnp.sum(group_prob * group_onehot, axis=1)
    chosen_logits = jnp.take_along_axis(expert_logits, routes, axis=1)
    paired_exp = jnp.exp(chosen_logits)
    paired = paired_exp / jnp.sum(paired_exp, axis=1, keepdims=True)
    return (group_prob, group_onehot, picked, paired)


def body(tokens, cotangent, routes, router_group, router_expert, gate_proj, up_proj, down_proj):
    tok_rows, model_width = tokens.shape
    top_count = routes.shape[1]
    groups = router_group.shape[1]
    experts = router_expert.shape[1]
    group_width = experts // groups
    capacity = tok_rows // group_width
    tp_count = lax.axis_size("tp")
    tp_index = lax.axis_index("tp")
    col_width = model_width // tp_count
    group_prob, group_onehot, picked, paired = router_forward(
        tokens, routes, router_group, router_expert
    )
    weights = (picked[:, None] * paired).astype(jnp.bfloat16)
    assigned = tok_rows * top_count
    flat_ids = routes.reshape(assigned)
    expert_onehot = (flat_ids[:, None] == jnp.arange(experts, dtype=jnp.int32)[None, :]).astype(
        jnp.int32
    )
    earlier = lax.cumsum(expert_onehot, axis=0) - expert_onehot
    ranking = jnp.sum(earlier * expert_onehot, axis=1)
    slot_index = flat_ids * capacity + ranking
    owners = (
        jnp.full((experts * capacity,), assigned, jnp.int32)
        .at[slot_index]
        .set(jnp.arange(assigned, dtype=jnp.int32))
    )
    source_rows = owners // top_count
    send_tokens = jnp.take(tokens, source_rows, axis=0, mode="fill", fill_value=0)
    send_cot = jnp.take(cotangent, source_rows, axis=0, mode="fill", fill_value=0)
    send_weight = jnp.take(weights.reshape(assigned), owners, axis=0, mode="fill", fill_value=0)
    col_start = tp_index * col_width
    part_tok = lax.dynamic_slice_in_dim(send_tokens, col_start, col_width, 1)
    part_cot = lax.dynamic_slice_in_dim(send_cot, col_start, col_width, 1)
    part_tok, part_cot, got_weight = (
        lax.all_to_all(part_tok, "ep", split_axis=0, concat_axis=0, tiled=True),
        lax.all_to_all(part_cot, "ep", split_axis=0, concat_axis=0, tiled=True),
        lax.all_to_all(send_weight, "ep", split_axis=0, concat_axis=0, tiled=True),
    )
    inputs, upstream = (
        lax.all_gather(part_tok, "tp", axis=1, tiled=True),
        lax.all_gather(part_cot, "tp", axis=1, tiled=True),
    )
    slot_scale = got_weight.astype(jnp.float32)
    gate_mat = gate_proj[0]
    up_mat = up_proj[0]
    down_mat = down_proj[0]
    gate_pre = jnp.dot(inputs, gate_mat, preferred_element_type=jnp.float32)
    up_pre = jnp.dot(inputs, up_mat, preferred_element_type=jnp.float32)
    sigmoid_gate = jax.nn.sigmoid(gate_pre)
    hidden = (gate_pre * sigmoid_gate * up_pre).astype(jnp.bfloat16)
    pulled = contract_cols(upstream, down_mat)
    weight_part = jnp.sum(pulled * hidden.astype(jnp.float32), axis=1)
    dhidden = slot_scale[:, None] * pulled
    gate_delta = (dhidden * up_pre * sigmoid_gate * (1.0 + gate_pre * (1.0 - sigmoid_gate))).astype(
        jnp.bfloat16
    )
    up_delta = (dhidden * gate_pre * sigmoid_gate).astype(jnp.bfloat16)
    scaled_cot = (slot_scale[:, None] * upstream.astype(jnp.float32)).astype(jnp.bfloat16)
    gate_total = contract_rows(inputs, gate_delta)
    up_total = contract_rows(inputs, up_delta)
    down_total = contract_rows(hidden, scaled_cot)
    token_term = contract_cols(gate_delta, gate_mat) + contract_cols(up_delta, up_mat)
    token_sum = lax.psum_scatter(
        token_term.astype(jnp.bfloat16), "tp", scatter_dimension=1, tiled=True
    )
    weight_sum, gate_sq, up_sq = lax.psum(
        (
            weight_part,
            jnp.sum(gate_total * gate_total, axis=1),
            jnp.sum(up_total * up_total, axis=1),
        ),
        "tp",
    )
    returned, weight_back = (
        lax.all_to_all(token_sum, "ep", split_axis=0, concat_axis=0, tiled=True),
        lax.all_to_all(
            weight_sum.astype(jnp.bfloat16), "ep", split_axis=0, concat_axis=0, tiled=True
        ),
    )
    back_rows = jnp.take(returned, slot_index, axis=0)
    expert_part = jnp.sum(
        back_rows.reshape(tok_rows, top_count, col_width).astype(jnp.float32), axis=1
    )
    dweight = jnp.take(weight_back, slot_index, axis=0).astype(jnp.float32)
    dweight = dweight.reshape(tok_rows, top_count)
    dpicked = jnp.sum(dweight * paired, axis=1)
    dpaired = dweight * picked[:, None]
    dchosen = paired * (dpaired - jnp.sum(paired * dpaired, axis=1, keepdims=True))
    dgroup = ((dpicked * picked)[:, None] * (group_onehot - group_prob)).astype(jnp.bfloat16)
    route_onehot = (
        routes[:, :, None] == jnp.arange(experts, dtype=jnp.int32)[None, None, :]
    ).astype(jnp.float32)
    dexpert = jnp.sum(dchosen[:, :, None] * route_onehot, axis=1).astype(jnp.bfloat16)
    own_cols = tp_index * col_width
    group_cols = lax.dynamic_slice_in_dim(router_group, own_cols, col_width, 0)
    expert_cols = lax.dynamic_slice_in_dim(router_expert, own_cols, col_width, 0)
    router_part = contract_cols(dgroup, group_cols) + contract_cols(dexpert, expert_cols)
    token_grad = (expert_part + router_part).astype(jnp.bfloat16)
    row_count = tok_rows // tp_count
    row_start = tp_index * row_count
    own_tokens = lax.dynamic_slice_in_dim(tokens, row_start, row_count, 0)
    expert_term = contract_rows(
        own_tokens, lax.dynamic_slice_in_dim(dexpert, row_start, row_count, 0)
    )
    group_term = contract_rows(
        own_tokens, lax.dynamic_slice_in_dim(dgroup, row_start, row_count, 0)
    )
    router_expert_grad, router_group_grad = (
        lax.psum_scatter(expert_term, ("ep", "tp"), scatter_dimension=0, tiled=True),
        lax.psum_scatter(group_term, ("ep", "tp"), scatter_dimension=0, tiled=True),
    )
    router_rows = jnp.sum(router_expert_grad * router_expert_grad, axis=1) + jnp.sum(
        router_group_grad * router_group_grad, axis=1
    )
    down_sq = jnp.sum(down_total * down_total, axis=1)
    return (
        token_grad,
        gate_total.astype(jnp.bfloat16)[None],
        up_total.astype(jnp.bfloat16)[None],
        down_total.astype(jnp.bfloat16)[None],
        gate_sq[None],
        up_sq[None],
        down_sq[None],
        router_expert_grad,
        router_group_grad,
        router_rows,
    )


def solution(mesh):
    return jax.shard_map(
        body,
        mesh=mesh,
        in_specs=(
            P("ep", None),
            P("ep", None),
            P("ep", None),
            P(),
            P(),
            P("ep", None, "tp"),
            P("ep", None, "tp"),
            P("ep", "tp", None),
        ),
        out_specs=(
            P("ep", "tp"),
            P("ep", None, "tp"),
            P("ep", None, "tp"),
            P("ep", "tp", None),
            P("ep", None),
            P("ep", None),
            P("ep", "tp"),
            P(("ep", "tp"), None),
            P(("ep", "tp"), None),
            P(("ep", "tp")),
        ),
        check_vma=False,
    )
```

profile of v0, /device:TPU:0, one launch (start us, length us, event | category | flops | bytes accessed | tf_op | source)
XLA Modules:
  0.0 438.0 jit_solution(13447635716263064559)
XLA Ops:
  7.2 0.8 broadcast_multiply_fusion
  8.0 0.8 copy.63
  8.8 0.1 eq.54
  8.9 0.1 reshape.163
  9.1 0.1 copy.68
  9.2 0.1 mul.144
  9.3 0.6 reduce-window.6
  9.9 0.2 slice_reduce_fusion
  10.2 0.1 fusion.21
  10.3 1.4 scatter_custom_fusion
  11.7 6.4 %gather_fusion.5 = bf16[512,2048]{1,0:T(8,128)(2,1)} fusion(bf16[128,2048]{1,0:T(8,128)(2,1)} %param.10, s32[1024]{0:T(1024)S(1)} %pad_clamp_fusion.1), kind=kCustom, calls=%fused_computation.1.clone | custom fusion | bytes 4196352 | tf_op jit(solution)/shard_map/jit(_take)/gather | solution.py:65
  18.1 3.3 gather_fusion.4
  21.5 2.9 dynamic-slice_select_fusion.1
  24.4 34.6 %all_to_all.55 = bf16[16,32,1024]{2,1,0:T(8,128)(2,1)} all-to-all(bf16[16,32,1024]{2,1,0:T(8,128)(2,1)S(1)} %bitcast.77), channel_id=1, replica_groups=mesh['ep'=16,'tp'=2] {'ep'}, dimensions={0} | all-to-all | bytes 2097152 | tf_op jit(solution)/shard_map/all_to_all | solution.py:72
  59.0 4.1 all-to-all-start.1
  63.1 0.0 all-gather.3.cloned.1.call-start
  63.2 0.3 fusion.42
  63.4 0.2 fusion.43
  63.7 23.1 %all-to-all-done.1 = bf16[16,32,1024]{2,1,0:T(8,128)(2,1)S(1)} async-done(((bf16[16,32,1024]{2,1,0:T(8,128)(2,1)}), bf16[16,32,1024]{2,1,0:T(8,128)(2,1)S(1)}, u32[]{:S(2)}, u32[]{:S(2)}) %all-to-all-start.1) | async-done | bytes 1048608 | tf_op jit(solution)/shard_map/all_to_all | solution.py:73
  86.8 1.0 copy-done.3
  87.8 0.1 copy.69
  87.9 0.1 reshape.207
  88.1 2.0 gather_fusion.3
  90.1 0.1 reshape.210
  90.2 0.1 copy.70
  90.3 0.1 copy.71
  90.5 0.2 mul.148
  90.7 3.4 gather_fusion
  94.1 0.1 select_n.106
  94.2 13.1 %all_to_all.56 = bf16[16,32,1]{1,2,0:T(2,128)(2,1)S(1)} all-to-all(bf16[16,32,1]{1,2,0:T(2,128)(2,1)S(1)} %select_n.106), channel_id=1, replica_groups=mesh['ep'=16,'tp'=2] {'ep'}, dimensions={0} | all-to-all | bytes 2048 | tf_op jit(solution)/shard_map/all_to_all | solution.py:74
  107.3 0.1 reshape.166
  107.4 3.3 fusion.6
  110.7 1.6 fusion.9
  112.2 3.1 multiply_reduce_fusion.3
  115.3 0.8 fusion.4
  116.1 2.2 add_convert_fusion
  118.3 3.4 convert_bitcast_fusion.2
  121.7 1.7 convert_bitcast_fusion.1
  123.4 4.0 all-reduce
  127.4 0.1 all_to_all.49
  127.5 9.9 %all_to_all.57 = bf16[16,32,1]{1,2,0:T(2,128)(2,1)S(1)} all-to-all(bf16[16,32,1]{1,2,0:T(2,128)(2,1)S(1)} %all_to_all.49), channel_id=1, replica_groups=mesh['ep'=16,'tp'=2] {'ep'}, dimensions={0} | all-to-all | bytes 2048 | tf_op jit(solution)/shard_map/all_to_all | solution.py:113
  137.4 3.7 all-to-all-start.3
  141.1 0.1 reduce_sum.131
  141.2 0.1 copy.66
  141.3 2.3 copy.76
  143.6 2.3 copy.75
  145.8 4.0 multiply_reduce_fusion
  149.8 0.1 all_to_all.48
  149.9 1.9 gather_fusion.2
  151.8 0.2 gather.28
  152.0 0.1 copy.74
  152.2 1.4 fusion.13
  153.7 1.4 fusion.15
  155.0 0.1 copy.67
  155.2 0.2 fusion.17
  155.4 136.2 %reduce-scatter.12.cloned.1.call-done = f32[64,4]{1,0:T(8,128)} async-done(((f32[2048,4]{1,0:T(8,128)}), f32[64,4]{1,0:T(8,128)}) %reduce-scatter.12.cloned.1.call-update) | async-done | bytes 1040
  291.6 0.8 copy.80
  292.5 133.8 %reduce-scatter.10.cloned.1.call-done = f32[64,16]{1,0:T(8,128)} async-done(((f32[2048,16]{1,0:T(8,128)}), f32[64,16]{1,0:T(8,128)}) %reduce-scatter.10.cloned.1.call-update) | async-done | bytes 4112
  426.3 0.8 copy.78
  427.1 0.5 add.125
  427.6 1.2 gather_fusion.1
  428.8 0.2 gather.26
  429.0 1.5 convert_reduce_fusion
  430.5 1.0 fusion.3
  (61 shorter events, 0.7 us)
Async XLA Ops:
  7.2 100.2 %copy-start = (bf16[1,2048,256]{2,1,0:T(8,128)(2,1)S(1)}, bf16[1,2048,256]{2,1,0:T(8,128)(2,1)}, u32[]{:S(2)}) copy-start(bf16[1,2048,256]{2,1,0:T(8,128)(2,1)} %param.15) | copy-start | bytes 3145732
  7.2 100.2 %all-gather.5.cloned.1.call-start = ((), (), s32[]{:S(2)}) async-start(), calls=%async_computation.9 | async-start | bytes 3145728 | tf_op jit(solution)/shard_map/all_gather | solution.py:77
  11.7 6.4 %copy-start.2 = (bf16[128,2048]{1,0:T(8,128)(2,1)S(1)}, bf16[128,2048]{1,0:T(8,128)(2,1)}, u32[]{:S(2)}) copy-start(bf16[128,2048]{1,0:T(8,128)(2,1)} %param.11) | copy-start | bytes 1572868
  58.9 4.2 copy-start.1
  58.9 4.2 copy-start.6
  58.9 4.5 %copy-start.5 = (bf16[2048,16]{0,1:T(8,128)(2,1)S(1)}, bf16[2048,16]{0,1:T(8,128)(2,1)}, u32[]{:S(2)}) copy-start(bf16[2048,16]{0,1:T(8,128)(2,1)} %param.14) | copy-start | bytes 196612
  59.0 28.8 %copy-start.7 = (s32[128,2]{0,1:T(2,128)S(1)}, s32[128,2]{0,1:T(2,128)}, u32[]{:S(2)}) copy-start(s32[128,2]{0,1:T(2,128)} %param.12) | copy-start | bytes 3076
  59.0 27.8 %all-to-all-start.1 = ((bf16[16,32,1024]{2,1,0:T(8,128)(2,1)}), bf16[16,32,1024]{2,1,0:T(8,128)(2,1)S(1)}, u32[]{:S(2)}, u32[]{:S(2)}) async-start(bf16[16,32,1024]{2,1,0:T(8,128)(2,1)} %bitcast.5), calls=%async_computation.1 | async-start | bytes 2097152 | tf_op jit(solution)/shard_map/all_to_all | solution.py:73
  63.1 49.1 %all-gather.3.cloned.1.call-start = ((), (), s32[]{:S(2)}) async-start(), calls=%async_computation.8 | async-start | bytes 3145728 | tf_op jit(solution)/shard_map/all_gather | solution.py:78
  86.8 1.0 copy-start.3
  87.7 49.6 %reduce-scatter.8.cloned.1.call-start = ((), (), s32[]{:S(2)}) async-start(), calls=%async_computation.10 | async-start | bytes 3145728 | tf_op jit(solution)/shard_map/reduce_scatter | solution.py:100
  94.0 16.6 %copy-start.4 = (bf16[1,2048,256]{2,1,0:T(8,128)(2,1)S(1)}, bf16[1,2048,256]{2,1,0:T(8,128)(2,1)}, u32[]{:S(2)}) copy-start(bf16[1,2048,256]{2,1,0:T(8,128)(2,1)} %param.16) | copy-start | bytes 3145732
  107.4 3.3 copy-start.10
  118.3 3.4 copy-start.11
  137.4 290.3 %all-to-all-start.3 = ((bf16[16,32,1024]{2,1,0:T(8,128)(2,1)}), bf16[16,32,1024]{2,1,0:T(8,128)(2,1)S(1)}, u32[]{:S(2)}, u32[]{:S(2)}) async-start(bf16[16,32,1024]{2,1,0:T(8,128)(2,1)} %bitcast.80), calls=%async_computation.4 | async-start | bytes 2097152 | tf_op jit(solution)/shard_map/all_to_all | solution.py:112
  141.0 150.6 %reduce-scatter.12.cloned.1.call-start = ((), (), s32[]{:S(2)}) async-start(), calls=%async_computation.12 | async-start | bytes 1081344
  153.6 272.7 %reduce-scatter.10.cloned.1.call-start = ((), (), s32[]{:S(2)}) async-start(), calls=%async_computation.11 | async-start | bytes 1081344
  292.4 136.3 %copy-start.9 = (f32[64,4]{0,1:T(4,128)}, f32[64,4]{0,1:T(4,128)S(1)}, u32[]{:S(2)}) copy-start(f32[64,4]{0,1:T(4,128)S(1)} %copy.80) | copy-start | bytes 3076
  427.1 1.7 copy-start.8
Sparse Core Ops, SparseCore 0:
  59.1 8.8 all-gather.4
  87.9 10.8 all-gather.2
  118.4 5.9 reduce-scatter.7
  153.7 137.8 reduce-scatter.11
  293.7 132.4 reduce-scatter.9
where the time goes:
time: 439 us; the launch traced here: 438 us
  waiting for transfers between devices  293 us (67%)
  blocking collectives  61.5 us (14%)
  local copies, waits for them, and re-layouts  30.1 us (7%)
  matrix products  24.5 us (6%)
  between operations  14.1 us (3%)
  starting transfers between devices  7.95 us (2%)
  other arithmetic  6.71 us (2%)
    unnamed x7, waiting for transfers between devices  270 us
    all_to_all x1, blocking collectives, body(): lax.all_to_all(part_tok, 'ep', split_axis=0, concat_axis=0, tiled=True)  34.6 us
    all_to_all x1, waiting for transfers between devices, body(): lax.all_to_all(part_cot, 'ep', split_axis=0, concat_axis=0, tiled=True)  23.1 us
    all_to_all x1, blocking collectives, body(): lax.all_to_all(send_weight, 'ep', split_axis=0, concat_axis=0, tiled=True)  13.1 us
    all_to_all x1, blocking collectives, body(): lax.all_to_all(weight_sum.astype(jnp.bfloat16), 'ep', split_axis=0, conca...  9.87 us
    dot_general x3, matrix products, contract_rows(): lax.dot_general(left_side, right_side, (((0,), (0,)), ((), ())), preferre...  9.08 us
  transfers between devices with their start and end apart: 7, of which 3 were waited for; matrix products, arithmetic and copies ran while one was open for 8% of the time, Pallas kernels for 0%

commit v1 on v0

v1 whole, which is shorter than its diff:
```python
import functools

import jax
import jax.numpy as jnp
from jax import lax
from jax.experimental import pallas as pl
from jax.experimental.pallas import tpu as pltpu
from jax.sharding import PartitionSpec as P

MESH = pl.DeviceIdType.MESH
BF = jnp.bfloat16
F32 = jnp.float32
TINY = 2.0**-126


def mm(a, b, da=1, db=0):
    return lax.dot_general(a, b, (((da,), (db,)), ((), ())), preferred_element_type=F32)


def lanes_of(shape, dim=1):
    return lax.broadcasted_iota(jnp.int32, shape, dim)


class Sizes:
    pass


def sizes_of(mesh, tokens, routes, router_group, router_expert, gate_proj):
    z = Sizes()
    z.n_ep, z.n_tp = mesh["ep"], mesh["tp"]
    z.rows, z.width = tokens.shape
    z.top = routes.shape[1]
    z.groups, z.experts = router_group.shape[1], router_expert.shape[1]
    z.gs = z.experts // z.groups
    z.cap = z.rows // z.gs
    z.gr = z.gs * z.cap // z.top
    z.r1 = z.groups * z.gr
    z.sl = z.groups * z.cap
    z.pairs = z.gs * z.sl
    z.ff = gate_proj.shape[2]
    z.cw = z.width // z.n_tp
    z.half_chunks = 2
    z.nc = 2 * z.half_chunks
    z.cc = z.cw // z.half_chunks
    z.rl = -(-(z.experts + z.groups) // 128) * 128
    z.rw = -(-(z.experts + z.groups) // 8) * 8
    z.ch = z.width // z.n_ep
    z.reduce_here = z.ch % 128 == 0 and z.n_ep % 2 == 0
    assert z.experts == z.n_ep and z.n_tp == 2 and z.top == 2
    assert z.sl & (z.sl - 1) == 0 and z.gr & (z.gr - 1) == 0
    return z


def kernel(
    z, tok_ref, cot_ref, routes_ref, rc_ref, gate_ref, up_ref, down_ref,
    tg_out, gate_out, up_out, down_out, gsq_out, usq_out, dsq_out, rout_out,
    s_mat, t_mat, s1m, r1m, s1, r1, s2m, x2m, s2, x2, y2m, y2,
    gacc, uacc, pacc, dcat, hid, wcol, wp, wpr, pts, ptr, pto,
    s3m, r3m, s3, r3, s4m, r4m, s4, r4, sq, sqr, term, trec, tsum, tsumr,
    z1s, z1r, p2s, p2r, fs, fr, ptsm, ptrm, r3s, r3r, r4s, r4r, ms, mr, ts, tr,
):
    e, t = lax.axis_index("ep"), lax.axis_index("tp")
    g, p = e // z.gs, e % z.gs
    other = 1 - t

    def rcopy(src, dst, ss, rs, ep, tp):
        return pltpu.make_async_remote_copy(
            src_ref=src, dst_ref=dst, send_sem=ss, recv_sem=rs,
            device_id=(ep, tp), device_id_type=MESH,
        )

    barrier = pltpu.get_barrier_semaphore()
    for d in range(1, z.n_ep):
        pl.semaphore_signal(
            barrier, inc=1, device_id=((e + d) % z.n_ep, t), device_id_type=MESH
        )
    pl.semaphore_signal(barrier, inc=1, device_id=(e, other), device_id_type=MESH)

    sends = []

    def grows(h):
        return pl.ds(pl.multiple_of(h * z.gr, z.gr), z.gr)

    def prows(q):
        return pl.ds(pl.multiple_of(q * z.sl, z.sl), z.sl)

    def group_send(src, dst, ss, rs, c):
        for d in range(1, z.groups):
            h = (g + d) % z.groups
            cp = rcopy(src.at[grows(h)], dst.at[grows(g)], ss.at[c, d], rs.at[c, d], h * z.gs + p, t)
            cp.start()
            sends.append(cp)
        dst[grows(g), :] = src[grows(g), :]

    def group_wait(src, dst, ss, rs, c):
        for d in range(1, z.groups):
            h = (g + z.groups - d) % z.groups
            rcopy(src.at[grows(h)], dst.at[grows(h)], ss.at[c, d], rs.at[c, d], h * z.gs + p, t).wait_recv()

    def plane_send(src, dst, ss, rs, c):
        for d in range(1, z.gs):
            q = (p + d) % z.gs
            cp = rcopy(src.at[prows(q)], dst.at[prows(p)], ss.at[c, d], rs.at[c, d], g * z.gs + q, t)
            cp.start()
            sends.append(cp)
        dst[prows(p), :] = src[prows(p), :]

    def plane_wait_one(src, dst, ss, rs, c, d):
        q = (p + z.gs - d) % z.gs
        rcopy(src.at[prows(q)], dst.at[prows(q)], ss.at[c, d], rs.at[c, d], g * z.gs + q, t).wait_recv()

    def plane_wait(src, dst, ss, rs, c):
        for d in range(1, z.gs):
            plane_wait_one(src, dst, ss, rs, c, d)

    def pair_send(src, dst, ss, rs):
        cp = rcopy(src, dst, ss, rs, e, other)
        cp.start()
        sends.append(cp)
        return cp

    tok = tok_ref[...]
    logits = mm(tok, rc_ref[...], 1, 1)
    lane = lanes_of((z.rows, z.rl))
    r0, r1_ = routes_ref[:, 0:1], routes_ref[:, 1:2]
    chosen = (lane == r0) | (lane == r1_)
    low = (lane - z.experts) * z.gs
    is_group = (lane >= z.experts) & (lane < z.experts + z.groups)
    in_group = is_group & (r0 >= low) & (r0 < low + z.gs)
    expd = jnp.exp(logits)
    gexp = jnp.where(is_group, expd, 0.0)
    gprob = gexp / jnp.sum(gexp, axis=1, keepdims=True)
    picked = jnp.sum(jnp.where(in_group, gprob, 0.0), axis=1, keepdims=True)
    pexp = jnp.where(chosen, expd, 0.0)
    paired = pexp / jnp.sum(pexp, axis=1, keepdims=True)
    meta = jnp.where(chosen, jnp.maximum(picked * paired, TINY), 0.0).astype(BF)

    def before(n):
        return (lanes_of((n, n), 1) < lanes_of((n, n), 0)).astype(F32).astype(BF)

    ghot = in_group.astype(F32)
    grank = mm(before(z.rows), ghot.astype(BF))
    grank = jnp.where(in_group, grank, -1.0).astype(BF)
    er, el = lanes_of((z.rl, z.r1), 0) - z.experts, lanes_of((z.rl, z.r1), 1)
    expand = ((el >= er * z.gr) & (el < (er + 1) * z.gr)).astype(F32).astype(BF)
    place = (lanes_of((z.rows, z.r1)) & (z.gr - 1)).astype(F32)
    s_mat[...] = (mm(grank, expand) == place).astype(F32).astype(BF)

    s1m[...] = mm(s_mat[...], meta, 0, 0).astype(BF)
    pl.semaphore_wait(barrier, z.n_ep)
    group_send(s1m, r1m, z1s, z1r, z.nc)

    def cols_at(half, k):
        return pl.ds(pl.multiple_of(half * z.cw + k * z.cc, z.cc), z.cc)

    for c in range(z.nc):
        src = tok_ref if c < z.half_chunks else cot_ref
        s1[c] = mm(s_mat[...], src[:, cols_at(t, c % z.half_chunks)], 0, 0).astype(BF)
        group_send(s1.at[c], r1.at[c], z1s, z1r, c)

    group_wait(s1m, r1m, z1s, z1r, z.nc)
    vals = r1m[...]
    lane1 = lanes_of((z.r1, z.rl))
    member = (vals.astype(F32) > 0.0) & (lane1 < z.experts)
    rank = mm(before(z.r1), member.astype(F32).astype(BF))
    rank = jnp.where(member, rank, -1.0).astype(BF)
    er, el = lanes_of((z.rl, z.pairs), 0) - g * z.gs, lanes_of((z.rl, z.pairs), 1)
    expand = ((el >= er * z.sl) & (el < (er + 1) * z.sl)).astype(F32).astype(BF)
    place = (lanes_of((z.r1, z.pairs)) & (z.sl - 1)).astype(F32)
    t_mat[...] = (mm(rank, expand) == place).astype(F32).astype(BF)
    s2m[...] = mm(t_mat[...], vals, 0, 0).astype(BF)
    plane_send(s2m, x2m, p2s, p2r, z.nc)

    def pack_two(c):
        group_wait(s1.at[c], r1.at[c], z1s, z1r, c)
        s2[c] = mm(t_mat[...], r1[c], 0, 0).astype(BF)
        plane_send(s2.at[c], x2.at[c], p2s, p2r, c)
        pair_send(x2.at[c, prows(p)], y2.at[c, prows(p)], fs.at[c, 0], fr.at[c, 0])

    def accumulate(x, half, c):
        if c < z.half_chunks:
            at = cols_at(half, c)
            gate_add, up_add = mm(x, gate_ref[at, :]), mm(x, up_ref[at, :])
            gacc[...] += gate_add
            uacc[...] += up_add
        else:
            pacc[...] += mm(x, down_ref[:, cols_at(half, c - z.half_chunks)], 1, 1)

    def land(c):
        for d in range(1, z.gs):
            plane_wait_one(s2.at[c], x2.at[c], p2s, p2r, c, d)
            q = (p + z.gs - d) % z.gs
            pair_send(x2.at[c, prows(q)], y2.at[c, prows(q)], fs.at[c, d], fr.at[c, d])
        accumulate(x2[c], t, c)

    def land_other(c):
        for d in range(z.gs):
            q = (p + z.gs - d) % z.gs
            rcopy(x2.at[c, prows(q)], y2.at[c, prows(q)], fs.at[c, d], fr.at[c, d], e, other).wait_recv()
        accumulate(y2[c], other, c)

    gacc[...] = jnp.zeros_like(gacc)
    uacc[...] = jnp.zeros_like(uacc)
    pacc[...] = jnp.zeros_like(pacc)
    for c in range(z.nc + 2):
        if c < z.nc:
            pack_two(c)
        if 1 <= c <= z.nc:
            land(c - 1)
        if c >= 2:
            land_other(c - 2)
    plane_wait(s2m, x2m, p2s, p2r, z.nc)

    lane2 = lanes_of((z.pairs, z.rl))
    val = jnp.sum(jnp.where(lane2 == e, x2m[...].astype(F32), 0.0), axis=1, keepdims=True)
    scale = jnp.where(val > TINY, val, 0.0)
    wcol[...] = jnp.broadcast_to(scale, wcol.shape)
    gate_pre, up_pre, pulled = gacc[...], uacc[...], pacc[...]
    sig = 1.0 / (1.0 + jnp.exp(-gate_pre))
    silu = gate_pre * sig
    hidden = (silu * up_pre).astype(BF)
    hid[...] = hidden
    wp[...] = jnp.broadcast_to(
        jnp.sum(pulled * hidden.astype(F32), axis=1, keepdims=True), wp.shape
    )
    w_copy = pair_send(wp, wpr, ms.at[0], mr.at[0])
    dh = scale * pulled
    dcat[:, : z.ff] = (dh * up_pre * sig * (1.0 + gate_pre * (1.0 - sig))).astype(BF)
    dcat[:, z.ff :] = (dh * silu).astype(BF)

    def token_term(half, k):
        at = cols_at(half, k)
        return (
            mm(dcat[:, : z.ff], gate_ref[at, :], 1, 1) + mm(dcat[:, z.ff :], up_ref[at, :], 1, 1)
        ).astype(BF)

    pt = []
    for k in range(z.half_chunks):
        pts[k] = token_term(other, k)
        pt.append(pair_send(pts.at[k], ptr.at[k], ptsm.at[k], ptrm.at[k]))
    w_copy.wait_recv()
    wsum = wp[:, 0:1] + wpr[:, 0:1]
    s3m[...] = jnp.where(lane2 == e, wsum, 0.0).astype(BF)
    plane_send(s3m, r3m, r3s, r3r, z.half_chunks)
    for k in range(z.half_chunks):
        pto[k] = token_term(t, k)
        pt[k].wait_recv()
        s3[k] = (pto[k].astype(F32) + ptr[k].astype(F32)).astype(BF)
        plane_send(s3.at[k], r3.at[k], r3s, r3r, k)

    ones_ff = jnp.ones((16, z.ff), BF)

    def gate_up_grads(xs, half, k):
        at = cols_at(half, k)
        total = mm(xs[k], dcat[...], 0, 0)
        gate_out[at, :] = total[:, : z.ff].astype(BF)
        up_out[at, :] = total[:, z.ff :].astype(BF)
        square = (total * total).astype(BF)
        sq[0:1, at] = mm(ones_ff, square[:, : z.ff], 1, 1)[0:1]
        sq[1:2, at] = mm(ones_ff, square[:, z.ff :], 1, 1)[0:1]

    def down_grads(xs, half, k):
        scaled = (wcol[:, 0:1] * xs[z.half_chunks + k].astype(F32)).astype(BF)
        total = mm(hid[...], scaled, 0, 0)
        down_out[:, cols_at(half, k)] = total.astype(BF)
        return mm(jnp.ones((16, z.cc), BF), (total * total).astype(BF), 1, 1)[0:1]

    def back_two(k):
        plane_wait(s3.at[k], r3.at[k], r3s, r3r, k)
        s4[k] = mm(t_mat[...], r3[k]).astype(BF)
        group_send(s4.at[k], r4.at[k], r4s, r4r, k)

    gate_up_grads(x2, t, 0)
    plane_wait(s3m, r3m, r3s, r3r, z.half_chunks)
    s4m[...] = mm(t_mat[...], r3m[...]).astype(BF)
    group_send(s4m, r4m, r4s, r4r, z.half_chunks)
    gate_up_grads(x2, t, 1)
    gate_up_grads(y2, other, 0)
    back_two(0)
    gate_up_grads(y2, other, 1)
    sq_copy = pair_send(sq, sqr, ms.at[1], mr.at[1])

    group_wait(s4m, r4m, r4s, r4r, z.half_chunks)
    dw = mm(s_mat[...], r4m[...])
    dpicked = jnp.sum(dw * paired, axis=1, keepdims=True)
    q = picked * dw
    dchosen = paired * (q - jnp.sum(paired * q, axis=1, keepdims=True))
    dgroup = jnp.where(is_group, (dpicked * picked) * (ghot - gprob), 0.0)
    dall = (dchosen + dgroup).astype(BF)
    dterm = dall[:, : z.rw] if z.rw < z.rl else dall
    tcopies = []
    if z.reduce_here:
        full = mm(dterm, tok_ref[...], 0, 0)
        for i in range(z.n_ep):
            term[i] = full[:, i * z.ch : (i + 1) * z.ch]

        def term_copy(m):
            to = (e + 2 * m + t) % z.n_ep
            return rcopy(term.at[to], trec.at[m], ts.at[m], tr.at[m], to, t)

        @pl.when(t == 0)
        def _():
            trec[0] = term[e]

        @pl.when(t == 1)
        def _():
            term_copy(0).start()

        for m in range(1, z.n_ep // 2):
            term_copy(m).start()
    else:
        row = lanes_of((z.rows, z.rl), 0)[:, : dterm.shape[1]]
        mine = (row >= t * (z.rows // 2)) & (row < (t + 1) * (z.rows // 2))
        dterm = jnp.where(mine, dterm.astype(F32), 0.0).astype(BF)
        rout_out[...] = mm(dterm, tok_ref[...], 0, 0)

    back_two(1)
    dsq = down_grads(x2, t, 0)
    dsq += down_grads(x2, t, 1)
    dsq += down_grads(y2, other, 0)

    if z.reduce_here:

        @pl.when(t == 1)
        def _():
            term_copy(0).wait_recv()

        for m in range(1, z.n_ep // 2):
            term_copy(m).wait_recv()
        acc = trec[0]
        for m in range(1, z.n_ep // 2):
            acc = acc + trec[m]
        tsum[...] = acc
        t_pair = pair_send(tsum, tsumr, ms.at[2], mr.at[2])
    dsq += down_grads(y2, other, 1)
    dsq_out[...] = dsq

    for k in range(z.half_chunks):
        group_wait(s4.at[k], r4.at[k], r4s, r4r, k)
        tg_out[:, k * z.cc : (k + 1) * z.cc] = (
            mm(s_mat[...], r4[k]) + mm(dall, rc_ref[:, cols_at(t, k)])
        ).astype(BF)
    sq_copy.wait_recv()
    gsq_out[...] = sq[0:1, :] + sqr[0:1, :]
    usq_out[...] = sq[1:2, :] + sqr[1:2, :]
    if z.reduce_here:
        t_pair.wait_recv()
        rout_out[...] = tsum[...] + tsumr[...]

        @pl.when(t == 1)
        def _():
            term_copy(0).wait_send()

        for m in range(1, z.n_ep // 2):
            term_copy(m).wait_send()
    for cp in sends:
        cp.wait_send()


def body(axes, tokens, cotangent, routes, router_group, router_expert, gate_proj, up_proj, down_proj):
    z = sizes_of(axes, tokens, routes, router_group, router_expert, gate_proj)
    rc = jnp.concatenate([router_expert.T, router_group.T], axis=0)
    rc = jnp.pad(rc, ((0, z.rl - rc.shape[0]), (0, 0)))
    h, nc, cc = z.half_chunks, z.nc, z.cc
    rout_shape = (z.rw, z.ch) if z.reduce_here else (min(z.rw, z.rl), z.width)
    outs = [
        ((z.rows, z.cw), BF), ((z.width, z.ff), BF), ((z.width, z.ff), BF), ((z.ff, z.width), BF),
        ((1, z.width), F32), ((1, z.width), F32), ((1, z.ff), F32), (rout_shape, F32),
    ]
    V = pltpu.VMEM
    chd = z.ch if z.reduce_here else 128
    scratch = [
        V((z.rows, z.r1), BF), V((z.r1, z.pairs), BF),
        V((z.r1, z.rl), BF), V((z.r1, z.rl), BF),
        V((nc, z.r1, cc), BF), V((nc, z.r1, cc), BF),
        V((z.pairs, z.rl), BF), V((z.pairs, z.rl), BF),
        V((nc, z.pairs, cc), BF), V((nc, z.pairs, cc), BF),
        V((8, 128), BF), V((nc, z.pairs, cc), BF),
        V((z.pairs, z.ff), F32), V((z.pairs, z.ff), F32), V((z.pairs, z.ff), F32),
        V((z.pairs, 2 * z.ff), BF), V((z.pairs, z.ff), BF), V((z.pairs, 128), F32),
        V((z.pairs, 128), F32), V((z.pairs, 128), F32),
        V((h, z.pairs, cc), BF), V((h, z.pairs, cc), BF), V((h, z.pairs, cc), BF),
        V((z.pairs, z.rl), BF), V((z.pairs, z.rl), BF),
        V((h, z.pairs, cc), BF), V((h, z.pairs, cc), BF),
        V((z.r1, z.rl), BF), V((z.r1, z.rl), BF),
        V((h, z.r1, cc), BF), V((h, z.r1, cc), BF),
        V((2, z.width), F32), V((2, z.width), F32),
        V((z.n_ep, z.rw, chd), F32), V((z.n_ep // 2, z.rw, chd), F32),
        V((z.rw, chd), F32), V((z.rw, chd), F32),
    ]
    D = pltpu.SemaphoreType.DMA
    sems = [
        D((nc + 1, z.groups)), D((nc + 1, z.groups)), D((nc + 1, z.gs)), D((nc + 1, z.gs)),
        D((nc, z.gs)), D((nc, z.gs)), D((h,)), D((h,)),
        D((h + 1, z.gs)), D((h + 1, z.gs)), D((h + 1, z.groups)), D((h + 1, z.groups)),
        D((3,)), D((3,)), D((z.n_ep // 2,)), D((z.n_ep // 2,)),
    ]
    spec = pl.BlockSpec(memory_space=pltpu.VMEM)
    tg, gate, up, down, gsq, usq, dsq, rout = pl.pallas_call(
        functools.partial(kernel, z),
        out_shape=[jax.ShapeDtypeStruct(s, d) for s, d in outs],
        in_specs=[spec] * 7,
        out_specs=[spec] * len(outs),
        scratch_shapes=scratch + sems,
        compiler_params=pltpu.CompilerParams(
            collective_id=0, has_side_effects=True, vmem_limit_bytes=60 * 2**20
        ),
    )(tokens, cotangent, routes, rc, gate_proj[0], up_proj[0], down_proj[0])
    own = z.width // (z.n_ep * z.n_tp)
    if z.reduce_here:
        mine = lax.dynamic_slice_in_dim(rout, lax.axis_index("tp") * own, own, 1).T
    else:
        mine = lax.psum_scatter(rout.T, ("ep", "tp"), scatter_dimension=0, tiled=True)
    reg = mine[:, : z.experts]
    rgg = mine[:, z.experts : z.experts + z.groups]
    rrows = jnp.sum(reg * reg, axis=1) + jnp.sum(rgg * rgg, axis=1)
    return (tg, gate[None], up[None], down[None], gsq, usq, dsq, reg, rgg, rrows)


def solution(mesh):
    return jax.shard_map(
        functools.partial(body, dict(mesh.shape)),
        mesh=mesh,
        in_specs=(
            P("ep", None), P("ep", None), P("ep", None), P(), P(),
            P("ep", None, "tp"), P("ep", None, "tp"), P("ep", "tp", None),
        ),
        out_specs=(
            P("ep", "tp"), P("ep", None, "tp"), P("ep", None, "tp"), P("ep", "tp", None),
            P("ep", None), P("ep", None), P("ep", "tp"),
            P(("ep", "tp"), None), P(("ep", "tp"), None), P(("ep", "tp")),
        ),
        check_vma=False,
    )
```

time: 439 us -> 90.5 us (0.21)
  waiting for transfers between devices: 293 us -> 0 us
  Pallas kernels: 0 us -> 74.8 us
  blocking collectives: 61.5 us -> 0 us
  matrix products: 24.5 us -> 0 us
  local copies, waits for them, and re-layouts: 30.1 us -> 9.98 us
  between operations: 14.1 us -> 0.68 us
  starting transfers between devices: 7.95 us -> 0 us
    unnamed x7 -> x0, waiting for transfers between devices: 270 us -> none
    pallas_call x0 -> x1, Pallas kernels: none -> 74.8 us  [body(): pl.pallas_call(functools.partial(kernel, z), out_shape=[jax.ShapeDtypeStr...]
    all_to_all x3 -> x0, blocking collectives: 57.5 us -> none  [the longest x1 34.6 us: body(): lax.all_to_all(part_tok, 'ep', split_axis=0, concat_axis=0, tiled=True)]
    all_to_all x2 -> x0, waiting for transfers between devices: 23.1 us -> none  [the longest x1 23.1 us: body(): lax.all_to_all(part_cot, 'ep', split_axis=0, concat_axis=0, tiled=True)]
    dot_general x12 -> x0, matrix products: 21.7 us -> none  [the longest x3 9.08 us: contract_rows(): lax.dot_general(left_side, right_side, (((0,), (0,)), ((), ())), preferre...]
    gather x13 -> x0, local copies, waits for them, and re-layouts: 19 us -> none  [the longest x1 6.4 us: body(): jnp.take(tokens, source_rows, axis=0, mode='fill', fill_value=0)]
    all_to_all x2 -> x0, starting transfers between devices: 7.74 us -> none  [the longest x1 4.09 us: body(): lax.all_to_all(part_cot, 'ep', split_axis=0, concat_axis=0, tiled=True)]
    unnamed x29 -> x22, local copies, waits for them, and re-layouts: 7.99 us -> 9.9 us
  transfers between devices with their start and end apart: 7 -> 0, of which waited for: 3 -> 0; matrix products, arithmetic and copies ran while one was open for 8% -> 0% of each run, Pallas kernels for 0% -> 0%
where the time goes in v1:
time: 90.5 us; the launch traced here: 88.9 us
  Pallas kernels  74.8 us (83%)
  local copies, waits for them, and re-layouts  9.98 us (11%)
  other arithmetic  3.4 us (4%)
    pallas_call x1, Pallas kernels, body(): pl.pallas_call(functools.partial(kernel, z), out_shape=[jax.ShapeDtypeStr...  74.8 us
    unnamed x22, local copies, waits for them, and re-layouts  9.9 us

profile of v1, /device:TPU:0, one launch (start us, length us, event | category | flops | bytes accessed | tf_op | source)
XLA Modules:
  0.0 88.9 jit_solution(4229859837781319409)
XLA Ops:
  0.6 0.0 copy-start.5
  0.7 1.7 %fusion.2.rc_ref = bf16[128,2048]{1,0:T(8,128)(2,1)} fusion(bf16[4,2048]{1,0:T(4,128)(2,1)} %bitcast.17, bf16[16,2048]{1,0:T(8,128)(2,1)} %bitcast.16), kind=kLoop, calls=%fused_computation.3 | loop fusion | flops 1835008 | bytes 606208 | tf_op jit(solution)/shard_map/concatenate | solution.py:362
  2.4 0.0 copy-done.5
  2.4 0.7 copy.18.routes_ref
  3.1 74.8 %shard_map.159 = (bf16[128,1024]{1,0:T(8,128)(2,1)}, bf16[2048,256]{1,0:T(8,128)(2,1)}, bf16[2048,256]{1,0:T(8,128)(2,1)}, bf16[256,2048]{1,0:T(8,128)(2,1)}, f3...) custom-call(bf16[128,2048]{1,0:T(8,128)(2,1)} %tok_ref.1, ...), custom_call_target="tpu_custom_call" | custom-call | tf_op jit(solution)/shard_map/pallas_call | solution.py:399
  77.9 0.0 copy-start.2
  78.0 0.7 copy-done.2
  78.7 0.1 dynamic-slice_bitcast_fusion
  78.7 0.6 multiply_reduce_fusion
  79.3 0.6 multiply_reduce_fusion.1
  79.9 0.5 add.9
  80.4 1.7 %copy.26 = bf16[128,1024]{1,0:T(8,128)(2,1)} copy(bf16[128,1024]{1,0:T(8,128)(2,1)} %get-tuple-element.40) | data formatting | bytes 524288
  82.1 0.0 copy-start.1
  82.1 2.4 %copy.27 = bf16[1,2048,256]{2,1,0:T(8,128)(2,1)} copy(bf16[1,2048,256]{2,1,0:T(8,128)(2,1)} %bitcast.12) | data formatting | bytes 2097152
  84.4 0.0 copy-done.1
  84.5 0.0 copy-start
  84.5 1.0 %copy.28 = bf16[1,2048,256]{2,1,0:T(8,128)(2,1)} copy(bf16[1,2048,256]{2,1,0:T(8,128)(2,1)S(1)} %bitcast.11) | data formatting | bytes 2097152
  85.4 0.6 copy-done
  86.1 0.0 copy-start.4
  86.1 1.0 %copy.29 = bf16[1,256,2048]{2,1,0:T(8,128)(2,1)} copy(bf16[1,256,2048]{2,1,0:T(8,128)(2,1)S(1)} %bitcast.10) | data formatting | bytes 2097152
  87.0 0.0 copy-done.4
  87.0 0.0 copy-start.3
  87.0 0.6 copy.30
  87.6 0.1 copy-done.3
  87.7 0.0 copy-start.6
  87.7 0.6 copy.31
  88.3 0.0 copy-done.6
  88.3 0.6 copy.32
Async XLA Ops:
  0.6 1.7 %copy-start.5 = (s32[128,2]{0,1:T(2,128)S(1)}, s32[128,2]{0,1:T(2,128)}, u32[]{:S(2)}) copy-start(s32[128,2]{0,1:T(2,128)} %param.10) | copy-start | bytes 3076
  77.9 0.7 copy-start.2
  82.1 2.4 %copy-start.1 = (bf16[2048,256]{1,0:T(8,128)(2,1)S(1)}, bf16[2048,256]{1,0:T(8,128)(2,1)}, u32[]{:S(2)}) copy-start(bf16[2048,256]{1,0:T(8,128)(2,1)} %get-tuple-element.20) | copy-start | bytes 3145732
  84.5 1.6 %copy-start = (bf16[256,2048]{1,0:T(8,128)(2,1)S(1)}, bf16[256,2048]{1,0:T(8,128)(2,1)}, u32[]{:S(2)}) copy-start(bf16[256,2048]{1,0:T(8,128)(2,1)} %get-tuple-element.21) | copy-start | bytes 3145732
  86.1 1.0 %copy-start.4 = (f32[1,2048]{1,0:T(1,128)S(1)}, f32[1,2048]{1,0:T(1,128)}, u32[]{:S(2)}) copy-start(f32[1,2048]{1,0:T(1,128)} %get-tuple-element.44) | copy-start | bytes 24580
  87.0 0.7 copy-start.3
  87.7 0.6 copy-start.6

commit v2 on v1

--- a/solution.py
+++ b/solution.py
@@ -10,7 +10,6 @@
 MESH = pl.DeviceIdType.MESH
 BF = jnp.bfloat16
 F32 = jnp.float32
-TINY = 2.0**-126
 
 
 def mm(a, b, da=1, db=0):
@@ -39,7 +38,7 @@
     z.pairs = z.gs * z.sl
     z.ff = gate_proj.shape[2]
     z.cw = z.width // z.n_tp
-    z.half_chunks = 2
+    z.half_chunks = 4
     z.nc = 2 * z.half_chunks
     z.cc = z.cw // z.half_chunks
     z.rl = -(-(z.experts + z.groups) // 128) * 128
@@ -52,8 +51,9 @@
 
 
 def kernel(
-    z, tok_ref, cot_ref, routes_ref, rc_ref, gate_ref, up_ref, down_ref,
+    z, tok_ref, cot_ref, routes_ref, rexp_ref, rgrp_ref, gate_ref, up_ref, down_ref,
     tg_out, gate_out, up_out, down_out, gsq_out, usq_out, dsq_out, rout_out,
+    rc_ref, s1w, r1w,
     s_mat, t_mat, s1m, r1m, s1, r1, s2m, x2m, s2, x2, y2m, y2,
     gacc, uacc, pacc, dcat, hid, wcol, wp, wpr, pts, ptr, pto,
     s3m, r3m, s3, r3, s4m, r4m, s4, r4, sq, sqr, term, trec, tsum, tsumr,
@@ -119,21 +119,17 @@
         sends.append(cp)
         return cp
 
-    tok = tok_ref[...]
-    logits = mm(tok, rc_ref[...], 1, 1)
     lane = lanes_of((z.rows, z.rl))
-    r0, r1_ = routes_ref[:, 0:1], routes_ref[:, 1:2]
+    eye = lanes_of((z.rows, z.rows), 0) == lanes_of((z.rows, z.rows), 1)
+
+    def column(row):
+        return jnp.sum(jnp.where(eye, row.astype(F32), 0.0), axis=1, keepdims=True).astype(jnp.int32)
+
+    r0, r1_ = column(routes_ref[0:1, :]), column(routes_ref[1:2, :])
     chosen = (lane == r0) | (lane == r1_)
     low = (lane - z.experts) * z.gs
     is_group = (lane >= z.experts) & (lane < z.experts + z.groups)
     in_group = is_group & (r0 >= low) & (r0 < low + z.gs)
-    expd = jnp.exp(logits)
-    gexp = jnp.where(is_group, expd, 0.0)
-    gprob = gexp / jnp.sum(gexp, axis=1, keepdims=True)
-    picked = jnp.sum(jnp.where(in_group, gprob, 0.0), axis=1, keepdims=True)
-    pexp = jnp.where(chosen, expd, 0.0)
-    paired = pexp / jnp.sum(pexp, axis=1, keepdims=True)
-    meta = jnp.where(chosen, jnp.maximum(picked * paired, TINY), 0.0).astype(BF)
 
     def before(n):
         return (lanes_of((n, n), 1) < lanes_of((n, n), 0)).astype(F32).astype(BF)
@@ -146,7 +142,7 @@
     place = (lanes_of((z.rows, z.r1)) & (z.gr - 1)).astype(F32)
     s_mat[...] = (mm(grank, expand) == place).astype(F32).astype(BF)
 
-    s1m[...] = mm(s_mat[...], meta, 0, 0).astype(BF)
+    s1m[...] = mm(s_mat[...], chosen.astype(F32).astype(BF), 0, 0).astype(BF)
     pl.semaphore_wait(barrier, z.n_ep)
     group_send(s1m, r1m, z1s, z1r, z.nc)
 
@@ -157,6 +153,18 @@
         src = tok_ref if c < z.half_chunks else cot_ref
         s1[c] = mm(s_mat[...], src[:, cols_at(t, c % z.half_chunks)], 0, 0).astype(BF)
         group_send(s1.at[c], r1.at[c], z1s, z1r, c)
+
+    rc_ref[...] = jnp.zeros_like(rc_ref)
+    rc_ref[0 : z.experts, :] = rexp_ref[...]
+    rc_ref[z.experts : z.experts + z.groups, :] = rgrp_ref[...]
+    expd = jnp.exp(mm(tok_ref[...], rc_ref[...], 1, 1))
+    gexp = jnp.where(is_group, expd, 0.0)
+    gprob = gexp / jnp.sum(gexp, axis=1, keepdims=True)
+    picked = jnp.sum(jnp.where(in_group, gprob, 0.0), axis=1, keepdims=True)
+    pexp = jnp.where(chosen, expd, 0.0)
+    paired = pexp / jnp.sum(pexp, axis=1, keepdims=True)
+    s1w[...] = mm(s_mat[...], (picked * paired).astype(BF), 0, 0).astype(BF)
+    group_send(s1w, r1w, z1s, z1r, z.nc + 1)
 
     group_wait(s1m, r1m, z1s, z1r, z.nc)
     vals = r1m[...]
@@ -168,8 +176,6 @@
     expand = ((el >= er * z.sl) & (el < (er + 1) * z.sl)).astype(F32).astype(BF)
     place = (lanes_of((z.r1, z.pairs)) & (z.sl - 1)).astype(F32)
     t_mat[...] = (mm(rank, expand) == place).astype(F32).astype(BF)
-    s2m[...] = mm(t_mat[...], vals, 0, 0).astype(BF)
-    plane_send(s2m, x2m, p2s, p2r, z.nc)
 
     def pack_two(c):
         group_wait(s1.at[c], r1.at[c], z1s, z1r, c)
@@ -202,18 +208,21 @@
     gacc[...] = jnp.zeros_like(gacc)
     uacc[...] = jnp.zeros_like(uacc)
     pacc[...] = jnp.zeros_like(pacc)
-    for c in range(z.nc + 2):
+    for c in range(z.nc + 3):
         if c < z.nc:
             pack_two(c)
-        if 1 <= c <= z.nc:
-            land(c - 1)
-        if c >= 2:
-            land_other(c - 2)
+        if c == z.nc - 1:
+            group_wait(s1w, r1w, z1s, z1r, z.nc + 1)
+            s2m[...] = mm(t_mat[...], r1w[...], 0, 0).astype(BF)
+            plane_send(s2m, x2m, p2s, p2r, z.nc)
+        if 2 <= c < z.nc + 2:
+            land(c - 2)
+        if c >= 3:
+            land_other(c - 3)
     plane_wait(s2m, x2m, p2s, p2r, z.nc)
 
     lane2 = lanes_of((z.pairs, z.rl))
-    val = jnp.sum(jnp.where(lane2 == e, x2m[...].astype(F32), 0.0), axis=1, keepdims=True)
-    scale = jnp.where(val > TINY, val, 0.0)
+    scale = jnp.sum(jnp.where(lane2 == e, x2m[...].astype(F32), 0.0), axis=1, keepdims=True)
     wcol[...] = jnp.broadcast_to(scale, wcol.shape)
     gate_pre, up_pre, pulled = gacc[...], uacc[...], pacc[...]
     sig = 1.0 / (1.0 + jnp.exp(-gate_pre))
@@ -275,10 +284,12 @@
     s4m[...] = mm(t_mat[...], r3m[...]).astype(BF)
     group_send(s4m, r4m, r4s, r4r, z.half_chunks)
     gate_up_grads(x2, t, 1)
-    gate_up_grads(y2, other, 0)
-    back_two(0)
-    gate_up_grads(y2, other, 1)
-    sq_copy = pair_send(sq, sqr, ms.at[1], mr.at[1])
+    for k in range(z.half_chunks - 1):
+        back_two(k)
+        if k + 2 < z.half_chunks:
+            gate_up_grads(x2, t, k + 2)
+        else:
+            gate_up_grads(y2, other, 0)
 
     group_wait(s4m, r4m, r4s, r4r, z.half_chunks)
     dw = mm(s_mat[...], r4m[...])
@@ -314,10 +325,13 @@
         dterm = jnp.where(mine, dterm.astype(F32), 0.0).astype(BF)
         rout_out[...] = mm(dterm, tok_ref[...], 0, 0)
 
-    back_two(1)
-    dsq = down_grads(x2, t, 0)
-    dsq += down_grads(x2, t, 1)
-    dsq += down_grads(y2, other, 0)
+    back_two(z.half_chunks - 1)
+    for k in range(1, z.half_chunks):
+        gate_up_grads(y2, other, k)
+    sq_copy = pair_send(sq, sqr, ms.at[1], mr.at[1])
+    dsq = jnp.zeros((1, z.ff), F32)
+    for k in range(z.half_chunks):
+        dsq += down_grads(x2, t, k)
 
     if z.reduce_here:
 
@@ -332,7 +346,8 @@
             acc = acc + trec[m]
         tsum[...] = acc
         t_pair = pair_send(tsum, tsumr, ms.at[2], mr.at[2])
-    dsq += down_grads(y2, other, 1)
+    for k in range(z.half_chunks):
+        dsq += down_grads(y2, other, k)
     dsq_out[...] = dsq
 
     for k in range(z.half_chunks):
@@ -357,10 +372,33 @@
         cp.wait_send()
 
 
+def finish(
+    z, gate_in, up_in, down_in, tg_in, gsq_in, usq_in, dsq_in, rout_in,
+    gate_out, up_out, down_out, tg_out, gsq_out, usq_out, dsq_out, reg_out, rgg_out, rows_out, sem,
+):
+    copies = []
+    pairs = (
+        (gate_in, gate_out), (up_in, up_out), (down_in, down_out), (tg_in, tg_out),
+        (gsq_in, gsq_out), (usq_in, usq_out), (dsq_in, dsq_out),
+    )
+    for i, (src, dst) in enumerate(pairs):
+        cp = pltpu.make_async_copy(src, dst, sem.at[i])
+        cp.start()
+        copies.append(cp)
+    half = z.ch // 2
+    both = rout_in[...]
+    mine = jnp.where(lax.axis_index("tp") == 0, both[:, :half], both[:, half:])
+    reg = mine[: z.experts]
+    rgg = mine[z.experts : z.experts + z.groups]
+    reg_out[...] = reg
+    rgg_out[...] = rgg
+    rows_out[...] = jnp.sum(reg * reg, axis=0, keepdims=True) + jnp.sum(rgg * rgg, axis=0, keepdims=True)
+    for cp in copies:
+        cp.wait()
+
+
 def body(axes, tokens, cotangent, routes, router_group, router_expert, gate_proj, up_proj, down_proj):
     z = sizes_of(axes, tokens, routes, router_group, router_expert, gate_proj)
-    rc = jnp.concatenate([router_expert.T, router_group.T], axis=0)
-    rc = jnp.pad(rc, ((0, z.rl - rc.shape[0]), (0, 0)))
     h, nc, cc = z.half_chunks, z.nc, z.cc
     rout_shape = (z.rw, z.ch) if z.reduce_here else (min(z.rw, z.rl), z.width)
     outs = [
@@ -370,6 +408,7 @@
     V = pltpu.VMEM
     chd = z.ch if z.reduce_here else 128
     scratch = [
+        V((z.rl, z.width), BF), V((z.r1, z.rl), BF), V((z.r1, z.rl), BF),
         V((z.rows, z.r1), BF), V((z.r1, z.pairs), BF),
         V((z.r1, z.rl), BF), V((z.r1, z.rl), BF),
         V((nc, z.r1, cc), BF), V((nc, z.r1, cc), BF),
@@ -390,7 +429,7 @@
     ]
     D = pltpu.SemaphoreType.DMA
     sems = [
-        D((nc + 1, z.groups)), D((nc + 1, z.groups)), D((nc + 1, z.gs)), D((nc + 1, z.gs)),
+        D((nc + 2, z.groups)), D((nc + 2, z.groups)), D((nc + 1, z.gs)), D((nc + 1, z.gs)),
         D((nc, z.gs)), D((nc, z.gs)), D((h,)), D((h,)),
         D((h + 1, z.gs)), D((h + 1, z.gs)), D((h + 1, z.groups)), D((h + 1, z.groups)),
         D((3,)), D((3,)), D((z.n_ep // 2,)), D((z.n_ep // 2,)),
@@ -399,21 +438,32 @@
     tg, gate, up, down, gsq, usq, dsq, rout = pl.pallas_call(
         functools.partial(kernel, z),
         out_shape=[jax.ShapeDtypeStruct(s, d) for s, d in outs],
-        in_specs=[spec] * 7,
+        in_specs=[spec] * 8,
         out_specs=[spec] * len(outs),
         scratch_shapes=scratch + sems,
         compiler_params=pltpu.CompilerParams(
-            collective_id=0, has_side_effects=True, vmem_limit_bytes=60 * 2**20
+            collective_id=0, has_side_effects=True, vmem_limit_bytes=44 * 2**20
         ),
-    )(tokens, cotangent, routes, rc, gate_proj[0], up_proj[0], down_proj[0])
-    own = z.width // (z.n_ep * z.n_tp)
+    )(tokens, cotangent, routes.T, router_expert.T, router_group.T, gate_proj[0], up_proj[0], down_proj[0])
     if z.reduce_here:
-        mine = lax.dynamic_slice_in_dim(rout, lax.axis_index("tp") * own, own, 1).T
+        half = z.ch // 2
+        shapes = [gate, up, down, tg, gsq, usq, dsq]
+        anywhere = pl.BlockSpec(memory_space=pl.ANY)
+        gate, up, down, tg, gsq, usq, dsq, reg, rgg, rrows = pl.pallas_call(
+            functools.partial(finish, z),
+            out_shape=[jax.ShapeDtypeStruct(a.shape, a.dtype) for a in shapes]
+            + [jax.ShapeDtypeStruct((n, half), F32) for n in (z.experts, z.groups, 1)],
+            in_specs=[spec] * 8,
+            out_specs=[anywhere] * 7 + [spec] * 3,
+            scratch_shapes=[D((7,))],
+            compiler_params=pltpu.CompilerParams(vmem_limit_bytes=16 * 2**20),
+        )(*shapes, rout)
+        reg, rgg, rrows = reg.T, rgg.T, rrows[0]
     else:
         mine = lax.psum_scatter(rout.T, ("ep", "tp"), scatter_dimension=0, tiled=True)
-    reg = mine[:, : z.experts]
-    rgg = mine[:, z.experts : z.experts + z.groups]
-    rrows = jnp.sum(reg * reg, axis=1) + jnp.sum(rgg * rgg, axis=1)
+        reg = mine[:, : z.experts]
+        rgg = mine[:, z.experts : z.experts + z.groups]
+        rrows = jnp.sum(reg * reg, axis=1) + jnp.sum(rgg * rgg, axis=1)
     return (tg, gate[None], up[None], down[None], gsq, usq, dsq, reg, rgg, rrows)
 
 

time: 90.5 us -> 82.5 us (0.912); the launches traced: 88.9 us -> 82 us
  other arithmetic: 3.4 us -> 0 us
  local copies, waits for them, and re-layouts: 9.98 us -> 7.98 us
  Pallas kernels: 74.8 us -> 73.2 us
    pallas_call x1, Pallas kernels: 74.8 us -> 70.8 us  [body(): pl.pallas_call(functools.partial(kernel, z), out_shape=[jax.ShapeDtypeStr...]
    pallas_call x0 -> x1, Pallas kernels: none -> 2.42 us  [body(): pl.pallas_call(functools.partial(finish, z), out_shape=[jax.ShapeDtypeStr...]
    unnamed x22 -> x16, local copies, waits for them, and re-layouts: 9.9 us -> 7.98 us
    concatenate x1 -> x0, other arithmetic: 1.7 us -> none  [body(): rc = jnp.concatenate([router_expert.T, router_group.T], axis=0)]
    reduce_sum x2 -> x0, other arithmetic: 1.18 us -> none  [body(): rrows = jnp.sum(reg * reg, axis=1) + jnp.sum(rgg * rgg, axis=1)]
where the time goes in v2:
time: 82.5 us; the launch traced here: 82 us
  Pallas kernels  73.2 us (89%)
  local copies, waits for them, and re-layouts  7.98 us (10%)
  between operations  0.83 us (1%)
    pallas_call x1, Pallas kernels, body(): pl.pallas_call(functools.partial(kernel, z), out_shape=[jax.ShapeDtypeStr...  70.8 us
    unnamed x16, local copies, waits for them, and re-layouts  7.98 us
    pallas_call x1, Pallas kernels, body(): pl.pallas_call(functools.partial(finish, z), out_shape=[jax.ShapeDtypeStr...  2.42 us

profile of v2, /device:TPU:0, one launch (start us, length us, event | category | flops | bytes accessed | tf_op | source)
XLA Modules:
  0.0 82.0 jit_solution(9604853336849357922)
XLA Ops:
  0.6 0.0 copy-start.7
  0.7 0.7 copy-done.7
  1.3 0.0 copy-start
  1.3 1.2 %copy-done = bf16[1,2048,256]{2,1,0:T(8,128)(2,1)S(1)} copy-done((bf16[1,2048,256]{2,1,0:T(8,128)(2,1)S(1)}, bf16[1,2048,256]{2,1,0:T(8,128)(2,1)}, u32[]{:S(2)}) %copy-start) | copy-done | bytes 1048600
  2.6 0.0 copy-start.1
  2.6 1.2 %copy-done.1 = bf16[1,2048,256]{2,1,0:T(8,128)(2,1)S(1)} copy-done((bf16[1,2048,256]{2,1,0:T(8,128)(2,1)S(1)}, bf16[1,2048,256]{2,1,0:T(8,128)(2,1)}, u32[]{:S(2)}) %copy-start.1) | copy-done | bytes 1048600
  3.8 0.0 copy-start.2
  3.8 1.2 %copy-done.2 = bf16[1,256,2048]{2,1,0:T(8,128)(2,1)S(1)} copy-done((bf16[1,256,2048]{2,1,0:T(8,128)(2,1)S(1)}, bf16[1,256,2048]{2,1,0:T(8,128)(2,1)}, u32[]{:S(2)}) %copy-start.2) | copy-done | bytes 1048600
  5.0 0.0 copy-start.3
  5.0 1.0 %copy-done.3 = bf16[128,2048]{1,0:T(8,128)(2,1)S(1)} copy-done((bf16[128,2048]{1,0:T(8,128)(2,1)S(1)}, bf16[128,2048]{1,0:T(8,128)(2,1)}, u32[]{:S(2)}) %copy-start.3) | copy-done | bytes 524312
  6.0 0.0 copy-start.4
  6.0 1.0 %copy-done.4 = bf16[128,2048]{1,0:T(8,128)(2,1)S(1)} copy-done((bf16[128,2048]{1,0:T(8,128)(2,1)S(1)}, bf16[128,2048]{1,0:T(8,128)(2,1)}, u32[]{:S(2)}) %copy-start.4) | copy-done | bytes 524312
  7.1 0.0 copy-start.5
  7.1 0.8 %copy-done.5 = bf16[2048,16]{0,1:T(8,128)(2,1)S(1)} copy-done((bf16[2048,16]{0,1:T(8,128)(2,1)S(1)}, bf16[2048,16]{0,1:T(8,128)(2,1)}, u32[]{:S(2)}) %copy-start.5) | copy-done | bytes 65560
  7.9 0.0 copy-start.6
  7.9 0.7 copy-done.6
  8.6 70.8 %shard_map.159 = (bf16[128,1024]{1,0:T(8,128)(2,1)S(1)}, bf16[2048,256]{1,0:T(8,128)(2,1)S(1)}, bf16[2048,256]{1,0:T(8,128)(2,1)S(1)}, bf16[256,2048]{1,0:T(8,12...) custom-call(bf16[128,2048]{1,0:T(8,128)(2,1)S(1)} %copy-done.3, ...), custom_call_target="tpu_custom_call" | custom-call | tf_op jit(solution)/shard_map/pallas_call | solution.py:438
  79.4 2.4 %shard_map.160 = (bf16[2048,256]{1,0:T(8,128)(2,1)}, bf16[2048,256]{1,0:T(8,128)(2,1)}, bf16[256,2048]{1,0:T(8,128)(2,1)}, bf16[128,1024]{1,0:T(8,128)(2,1)}, f3...) custom-call(bf16[2048,256]{1,0:T(8,128)(2,1)S(1)} %get-tuple-element, ...), custom_call_target="tpu_custom_call" | custom-call | tf_op jit(solution)/shard_map/pallas_call | solution.py:452
Async XLA Ops:
  0.6 0.7 copy-start.7
  1.3 1.2 %copy-start = (bf16[1,2048,256]{2,1,0:T(8,128)(2,1)S(1)}, bf16[1,2048,256]{2,1,0:T(8,128)(2,1)}, u32[]{:S(2)}) copy-start(bf16[1,2048,256]{2,1,0:T(8,128)(2,1)} %param.13) | copy-start | bytes 3145732
  2.6 1.2 %copy-start.1 = (bf16[1,2048,256]{2,1,0:T(8,128)(2,1)S(1)}, bf16[1,2048,256]{2,1,0:T(8,128)(2,1)}, u32[]{:S(2)}) copy-start(bf16[1,2048,256]{2,1,0:T(8,128)(2,1)} %param.14) | copy-start | bytes 3145732
  3.8 1.2 %copy-start.2 = (bf16[1,256,2048]{2,1,0:T(8,128)(2,1)S(1)}, bf16[1,256,2048]{2,1,0:T(8,128)(2,1)}, u32[]{:S(2)}) copy-start(bf16[1,256,2048]{2,1,0:T(8,128)(2,1)} %param.15) | copy-start | bytes 3145732
  5.0 1.0 %copy-start.3 = (bf16[128,2048]{1,0:T(8,128)(2,1)S(1)}, bf16[128,2048]{1,0:T(8,128)(2,1)}, u32[]{:S(2)}) copy-start(bf16[128,2048]{1,0:T(8,128)(2,1)} %tok_ref.1) | copy-start | bytes 1572868
  6.0 1.0 %copy-start.4 = (bf16[128,2048]{1,0:T(8,128)(2,1)S(1)}, bf16[128,2048]{1,0:T(8,128)(2,1)}, u32[]{:S(2)}) copy-start(bf16[128,2048]{1,0:T(8,128)(2,1)} %cot_ref.1) | copy-start | bytes 1572868
  7.1 0.8 %copy-start.5 = (bf16[2048,16]{0,1:T(8,128)(2,1)S(1)}, bf16[2048,16]{0,1:T(8,128)(2,1)}, u32[]{:S(2)}) copy-start(bf16[2048,16]{0,1:T(8,128)(2,1)} %param.12) | copy-start | bytes 196612
  7.9 0.7 copy-start.6
